TPU v7x, 32 devices: a whole 2x2x4 slice. The times are simulated.
32 devices in a mesh: grp: 1, ep: 16 (over z, y, x), tp: 2 (over core).
Axes of the slice: x: 2, y: 2, z: 4, core: 2. Of those that a mesh axis runs over, the one named last changes fastest.
Arguments:
- tokens_in: bfloat16 [1024, 2048], P(('grp', 'ep')), may hold values from -6 to 6
- norm_gain: float32 [2048], replicated, may hold values from 0.1 to 1.9
- gate_proj: bfloat16 [16, 2048, 1024], P('ep', None, 'tp'), may hold values from -0.125 to 0.125
- up_proj: bfloat16 [16, 2048, 1024], P('ep', None, 'tp'), may hold values from -0.125 to 0.125
- down_proj: bfloat16 [16, 1024, 2048], P('ep', 'tp'), may hold values from -0.1875 to 0.1875
- route_ids: int32 [1024, 8], P(('grp', 'ep')), may hold values from 0 to 15, all different within a row; in each aligned block of 64 rows (0 to 63, 64 to 127, ...) at most 64 rows name the same one
- group_weight: float32 [1024, 2], P(('grp', 'ep')), may hold values from 0.05 to 1
- expert_weight: float32 [1024, 8], P(('grp', 'ep')), may hold values from 0.05 to 1
Outputs:
- expert_mix: bfloat16 [1024, 2048], P(('grp', 'ep'), 'tp')
Inputs may be any that keep to these rules, and one draw needn't show every extreme that they name: `route_ids`: each row names 8 different experts; within the rows of one index of ep no expert is named by more than 64 rows, a bound that some of them reach.
All inputs are finite; a program needn't handle non-finite values.
Results may differ from a plain program's by a relative error of at most 0.0077.
Values may be sent and summed in bfloat16 or wider, within the bound.
A program may use at most 64 MiB of HBM per device.

v0:
```python
import jax
import jax.numpy as jnp
from jax import lax
from jax.sharding import PartitionSpec as P

EXP_GRP = 8
EPSILON = 1e-06


def on_device(
    tokens_in, norm_gain, gate_proj, up_proj, down_proj, route_ids, group_weight, expert_weight
):
    token_count, model_width = tokens_in.shape
    expert_count = gate_proj.shape[0] * lax.axis_size("ep")
    lane_count = lax.axis_size("tp")
    lane_index = lax.axis_index("tp")
    share = token_count // lane_count
    own_rows = lax.dynamic_slice_in_dim(tokens_in, lane_index * share, share, 0)
    row_values = own_rows.astype(jnp.float32)
    inv_scale = lax.rsqrt(jnp.mean(row_values * row_values, axis=-1, keepdims=True) + EPSILON)
    normed = (row_values * inv_scale * norm_gain).astype(jnp.bfloat16)
    rows = lax.all_gather(normed, ("ep", "tp"), axis=0, tiled=True)
    experts = jnp.arange(expert_count, dtype=jnp.int32)
    share_of = expert_weight / jnp.sum(expert_weight, axis=1, keepdims=True)
    named = route_ids[:, :, None] == experts[None, None, :]
    chosen = jnp.sum(jnp.where(named, share_of[:, :, None], 0.0), axis=1)
    gates = chosen * jnp.repeat(group_weight, EXP_GRP, axis=1)
    all_gates = lax.all_gather(gates, "ep", axis=0, tiled=True)
    own_gate = lax.dynamic_slice_in_dim(all_gates, lax.axis_index("ep"), 1, 1)
    gate_acts = jnp.dot(rows, gate_proj[0], preferred_element_type=jnp.float32)
    up_acts = jnp.dot(rows, up_proj[0], preferred_element_type=jnp.float32)
    hidden = (jax.nn.silu(gate_acts) * up_acts).astype(jnp.bfloat16)
    partial_rows = jnp.dot(hidden, down_proj[0], preferred_element_type=jnp.float32)
    weighted = (partial_rows * own_gate).astype(jnp.bfloat16)
    halves = lax.psum_scatter(weighted, "tp", scatter_dimension=1, tiled=True)
    return lax.psum_scatter(halves, "ep", scatter_dimension=0, tiled=True)


def solution(mesh):
    in_specs = (
        P(("grp", "ep"), None),
        P(),
        P("ep", None, "tp"),
        P("ep", None, "tp"),
        P("ep", "tp", None),
        P(("grp", "ep"), None),
        P(("grp", "ep"), None),
        P(("grp", "ep"), None),
    )
    out_specs = P(("grp", "ep"), "tp")
    return jax.shard_map(
        on_device, mesh=mesh, in_specs=in_specs, out_specs=out_specs, check_vma=False
    )
```

profile of v0, /device:TPU:0, one launch (start us, length us, event | category | flops | bytes accessed | tf_op | source)
XLA Modules:
  0.0 194.1 jit_solution(4281065118066478844)
XLA Ops:
  6.5 0.0 copy-start
  6.5 0.0 all-gather.3.cloned.1.call-start
  6.5 1.2 fusion.9
  7.7 1.7 fusion.11
  9.4 0.0 all-gather.3.cloned.1.call-update
  9.4 0.0 reduce-scatter.3.cloned.1.call-start
  9.5 0.7 reduce_sum.28
  10.2 0.7 broadcast_divide_fusion
  10.9 0.7 select_reduce_fusion
  11.6 0.7 fusion.12
  12.3 43.3 %all-gather = f32[16,64,16]{1,2,0:T(8,128)S(1)} all-gather(f32[1,64,16]{1,2,0:T(8,128)S(1)} %fusion.12), channel_id=1, replica_groups=mesh['grp'=1,'ep'=16,'tp'=2] {'ep'}, dimensions={0}, use_global_device_ids=true | all-gather | bytes 69632 | tf_op jit(solution)/shard_map/all_gather | solution.py:28
  55.7 0.1 reshape.17
  55.8 19.2 %all-gather.3.cloned.1.call-done = bf16[1024,2048]{1,0:T(8,128)(2,1)} async-done(((bf16[32,2048]{1,0:T(8,128)(2,1)}), bf16[1024,2048]{1,0:T(8,128)(2,1)}) %all-gather.3.cloned.1.call-update) | async-done | bytes 4194320 | tf_op jit(solution)/shard_map/all_gather | solution.py:22
  75.0 6.6 %fusion.1 = f32[1024,512]{1,0:T(8,128)} fusion(bf16[1024,2048]{1,0:T(8,128)(2,1)} %all-gather.3.cloned.1.call-done, bf16[1,2048,512]{2,1,0:T(8,128)(2,1)} %param.11), kind=kOutput, calls=%fused_computation.2 | convolution fusion | flops 2147483648 | bytes 8388608 | tf_op jit(solution)/shard_map/dot_general | solution.py:31
  81.5 0.0 copy-done
  81.5 10.1 %multiply_convert_fusion = bf16[1024,2048]{1,0:T(8,128)(2,1)} fusion(f32[1024]{0:T(1024)S(1)} %bitcast.24, bf16[1,512,2048]{2,1,0:T(8,128)(2,1)S(1)} %copy-done, f32[1024,512]{1,0:T(8,128)} %fusion.1, bf16[1024,2048]{1,0:T(8,128)(2,1)} %all-gather.3.cloned.1.call-done, bf16[1,2048,512]{2,1,0:T(8,128)(2,1)} %param.10), kind=kOutput, calls=%fused_computation | convolution fusion | flops 4302307328 | bytes 14684160 | tf_op jit(solution)/shard_map/dot_general | solution.py:33
  91.6 0.0 reduce-scatter.3.cloned.1.call-update
  91.6 0.0 reduce-scatter.5.cloned.1.call-start
  91.7 10.8 %reduce-scatter.3.cloned.1.call-done = bf16[1024,1024]{1,0:T(8,128)(2,1)} async-done(((bf16[1024,2048]{1,0:T(8,128)(2,1)}), bf16[1024,1024]{1,0:T(8,128)(2,1)}) %reduce-scatter.3.cloned.1.call-update) | async-done | bytes 2097168 | tf_op jit(solution)/shard_map/reduce_scatter | solution.py:35
  102.4 0.0 reduce-scatter.5.cloned.1.call-update
  102.4 85.1 %reduce-scatter.5.cloned.1.call-done = bf16[64,1024]{1,0:T(8,128)(2,1)} async-done(((bf16[1024,1024]{1,0:T(8,128)(2,1)}), bf16[64,1024]{1,0:T(8,128)(2,1)}) %reduce-scatter.5.cloned.1.call-update) | async-done | bytes 131088 | tf_op jit(solution)/shard_map/reduce_scatter | solution.py:36
  (3 shorter events, 0.1 us)
Async XLA Ops:
  6.5 75.0 %copy-start = (bf16[1,512,2048]{2,1,0:T(8,128)(2,1)S(1)}, bf16[1,512,2048]{2,1,0:T(8,128)(2,1)}, u32[]{:S(2)}) copy-start(bf16[1,512,2048]{2,1,0:T(8,128)(2,1)} %param.12) | copy-start | bytes 6291460
  6.5 68.4 %all-gather.3.cloned.1.call-start = ((), (), s32[]{:S(2)}) async-start(), calls=%async_computation.2 | async-start | bytes 4325376 | tf_op jit(solution)/shard_map/all_gather | solution.py:22
  9.4 93.0 %reduce-scatter.3.cloned.1.call-start = ((), (), s32[]{:S(2)}) async-start(), calls=%async_computation.3 | async-start | bytes 6291456 | tf_op jit(solution)/shard_map/reduce_scatter | solution.py:35
  91.6 95.9 %reduce-scatter.5.cloned.1.call-start = ((), (), s32[]{:S(2)}) async-start(), calls=%async_computation.4 | async-start | bytes 2228224 | tf_op jit(solution)/shard_map/reduce_scatter | solution.py:36
Sparse Core Ops, SparseCore 0:
  10.2 64.7 all-gather.2
  91.7 10.6 reduce-scatter.2
  104.7 82.7 reduce-scatter.4
where the time goes:
time: 194 us
  waiting for transfers between devices  115 us (59%)
  blocking collectives  43.3 us (22%)
  matrix products  16.6 us (9%)
  between operations  13.1 us (7%)
  other arithmetic  5.67 us (3%)
    reduce_scatter x1, waiting for transfers between devices, on_device(): return lax.psum_scatter(halves, 'ep', scatter_dimension=0, tiled=True)  85.1 us
    all_gather x1, blocking collectives, on_device(): all_gates = lax.all_gather(gates, 'ep', axis=0, tiled=True)  43.3 us
    all_gather x1, waiting for transfers between devices, on_device(): rows = lax.all_gather(normed, ('ep', 'tp'), axis=0, tiled=True)  19.2 us
    reduce_scatter x1, waiting for transfers between devices, on_device(): halves = lax.psum_scatter(weighted, 'tp', scatter_dimension=1, tiled=True)  10.8 us
    dot_general x1, matrix products, on_device(): jnp.dot(hidden, down_proj[0], preferred_element_type=jnp.float32)  10.1 us
    dot_general x1, matrix products, on_device(): up_acts = jnp.dot(rows, up_proj[0], preferred_element_type=jnp.float32)  6.59 us
  transfers between devices with their start and end apart: 3, of which 3 were waited for; matrix products, arithmetic and copies ran while one was open for 2% of the time, Pallas kernels for 0%

commit v1 on v0

--- a/solution.py
+++ b/solution.py
@@ -25,7 +25,12 @@
     named = route_ids[:, :, None] == experts[None, None, :]
     chosen = jnp.sum(jnp.where(named, share_of[:, :, None], 0.0), axis=1)
     gates = chosen * jnp.repeat(group_weight, EXP_GRP, axis=1)
-    all_gates = lax.all_gather(gates, "ep", axis=0, tiled=True)
+    ring = [gates]
+    for hop in range(15):
+        ring.append(lax.ppermute(ring[-1], "ep", [(dev, (dev + 1) % 16) for dev in range(16)]))
+    all_gates = jnp.roll(
+        jnp.concatenate(ring[::-1], axis=0), (lax.axis_index("ep") + 1) * ring[0].shape[0], axis=0
+    )
     own_gate = lax.dynamic_slice_in_dim(all_gates, lax.axis_index("ep"), 1, 1)
     gate_acts = jnp.dot(rows, gate_proj[0], preferred_element_type=jnp.float32)
     up_acts = jnp.dot(rows, up_proj[0], preferred_element_type=jnp.float32)

time: 194 us -> 240 us (1.24)
  waiting for transfers between devices: 115 us -> 201 us
  blocking collectives: 43.3 us -> 0 us
  starting transfers between devices: 0.09 us -> 3.09 us
    ppermute x0 -> x15, waiting for transfers between devices: none -> 108 us  [on_device(): lax.ppermute(ring[-1], 'ep', [(dev, (dev + 1) % 16) for dev in range(16)])]
    all_gather x1 -> x0, blocking collectives: 43.3 us -> none  [on_device(): all_gates = lax.all_gather(gates, 'ep', axis=0, tiled=True)]
    all_gather x1, waiting for transfers between devices: 19.2 us -> 0.01 us  [on_device(): rows = lax.all_gather(normed, ('ep', 'tp'), axis=0, tiled=True)]
    ppermute x0 -> x15, starting transfers between devices: none -> 3 us  [on_device(): lax.ppermute(ring[-1], 'ep', [(dev, (dev + 1) % 16) for dev in range(16)])]
    reduce_scatter x1, waiting for transfers between devices: 10.8 us -> 7.84 us  [on_device(): halves = lax.psum_scatter(weighted, 'tp', scatter_dimension=1, tiled=True)]
  transfers between devices with their start and end apart: 3 -> 18, of which waited for: 3 -> 17; matrix products, arithmetic and copies ran while one was open for 2% -> 1% of each run, Pallas kernels for 0% -> 0%
where the time goes in v1:
time: 240 us; the launch traced here: 239 us
  waiting for transfers between devices  201 us (84%)
  matrix products  16.6 us (7%)
  between operations  13.1 us (5%)
  other arithmetic  5.67 us (2%)
  starting transfers between devices  3.09 us (1%)
    ppermute x15, waiting for transfers between devices, on_device(): lax.ppermute(ring[-1], 'ep', [(dev, (dev + 1) % 16) for dev in range(16)])  108 us
    reduce_scatter x1, waiting for transfers between devices, on_device(): return lax.psum_scatter(halves, 'ep', scatter_dimension=0, tiled=True)  85.1 us
    dot_general x1, matrix products, on_device(): jnp.dot(hidden, down_proj[0], preferred_element_type=jnp.float32)  10.1 us
    reduce_scatter x1, waiting for transfers between devices, on_device(): halves = lax.psum_scatter(weighted, 'tp', scatter_dimension=1, tiled=True)  7.84 us
    dot_general x1, matrix products, on_device(): up_acts = jnp.dot(rows, up_proj[0], preferred_element_type=jnp.float32)  6.55 us
  transfers between devices with their start and end apart: 18, of which 17 were waited for; matrix products, arithmetic and copies ran while one was open for 1% of the time, Pallas kernels for 0%

profile of v1, /device:TPU:0, one launch (start us, length us, event | category | flops | bytes accessed | tf_op | source)
XLA Modules:
  0.0 239.3 jit_solution(3165049475335349477)
XLA Ops:
  6.5 1.2 fusion.12
  7.7 1.7 fusion.14
  9.5 0.7 reduce_sum.28
  10.9 0.7 select_reduce_fusion
  12.3 3.0 %collective-permute-start = (f32[64,16]{0,1:T(8,128)S(1)}, f32[64,16]{0,1:T(8,128)S(1)}, u32[]{:S(2)}, u32[]{:S(2)}) collective-permute-start(f32[64,16]{0,1:T(8,128)S(1)} %bitcast_multiply_fusion), channel_id=1, source_target_pairs={{0,2},{2,4},{4,6},{6,8},{8,10},{10,12},{12,14},{14,16},{16,18},{18... | collective-permute-start | bytes 12296 | tf_op jit(solution)/shard_map/ppermute | solution.py:30
  15.3 5.6 %collective-permute-done = f32[64,16]{0,1:T(8,128)S(1)} collective-permute-done((f32[64,16]{0,1:T(8,128)S(1)}, f32[64,16]{0,1:T(8,128)S(1)}, u32[]{:S(2)}, u32[]{:S(2)}) %collective-permute-start) | collective-permute-done | bytes 4128 | tf_op jit(solution)/shard_map/ppermute | solution.py:30
  20.9 7.3 %collective-permute-done.1 = f32[64,16]{0,1:T(8,128)S(1)} collective-permute-done((f32[64,16]{0,1:T(8,128)S(1)}, f32[64,16]{0,1:T(8,128)S(1)}, u32[]{:S(2)}, u32[]{:S(2)}) %collective-permute-start.1) | collective-permute-done | bytes 4128 | tf_op jit(solution)/shard_map/ppermute | solution.py:30
  28.1 7.3 %collective-permute-done.2 = f32[64,16]{0,1:T(8,128)S(1)} collective-permute-done((f32[64,16]{0,1:T(8,128)S(1)}, f32[64,16]{0,1:T(8,128)S(1)}, u32[]{:S(2)}, u32[]{:S(2)}) %collective-permute-start.2) | collective-permute-done | bytes 4128 | tf_op jit(solution)/shard_map/ppermute | solution.py:30
  35.5 7.4 %collective-permute-done.3 = f32[64,16]{0,1:T(8,128)S(1)} collective-permute-done((f32[64,16]{0,1:T(8,128)S(1)}, f32[64,16]{0,1:T(8,128)S(1)}, u32[]{:S(2)}, u32[]{:S(2)}) %collective-permute-start.3) | collective-permute-done | bytes 4128 | tf_op jit(solution)/shard_map/ppermute | solution.py:30
  42.8 7.2 %collective-permute-done.4 = f32[64,16]{0,1:T(8,128)S(1)} collective-permute-done((f32[64,16]{0,1:T(8,128)S(1)}, f32[64,16]{0,1:T(8,128)S(1)}, u32[]{:S(2)}, u32[]{:S(2)}) %collective-permute-start.4) | collective-permute-done | bytes 4128 | tf_op jit(solution)/shard_map/ppermute | solution.py:30
  50.1 7.2 %collective-permute-done.5 = f32[64,16]{0,1:T(8,128)S(1)} collective-permute-done((f32[64,16]{0,1:T(8,128)S(1)}, f32[64,16]{0,1:T(8,128)S(1)}, u32[]{:S(2)}, u32[]{:S(2)}) %collective-permute-start.5) | collective-permute-done | bytes 4128 | tf_op jit(solution)/shard_map/ppermute | solution.py:30
  57.3 7.5 %collective-permute-done.6 = f32[64,16]{0,1:T(8,128)S(1)} collective-permute-done((f32[64,16]{0,1:T(8,128)S(1)}, f32[64,16]{0,1:T(8,128)S(1)}, u32[]{:S(2)}, u32[]{:S(2)}) %collective-permute-start.6) | collective-permute-done | bytes 4128 | tf_op jit(solution)/shard_map/ppermute | solution.py:30
  64.9 7.3 %collective-permute-done.7 = f32[64,16]{0,1:T(8,128)S(1)} collective-permute-done((f32[64,16]{0,1:T(8,128)S(1)}, f32[64,16]{0,1:T(8,128)S(1)}, u32[]{:S(2)}, u32[]{:S(2)}) %collective-permute-start.7) | collective-permute-done | bytes 4128 | tf_op jit(solution)/shard_map/ppermute | solution.py:30
  72.1 7.2 %collective-permute-done.8 = f32[64,16]{0,1:T(8,128)S(1)} collective-permute-done((f32[64,16]{0,1:T(8,128)S(1)}, f32[64,16]{0,1:T(8,128)S(1)}, u32[]{:S(2)}, u32[]{:S(2)}) %collective-permute-start.8) | collective-permute-done | bytes 4128 | tf_op jit(solution)/shard_map/ppermute | solution.py:30
  79.4 7.2 %collective-permute-done.9 = f32[64,16]{0,1:T(8,128)S(1)} collective-permute-done((f32[64,16]{0,1:T(8,128)S(1)}, f32[64,16]{0,1:T(8,128)S(1)}, u32[]{:S(2)}, u32[]{:S(2)}) %collective-permute-start.9) | collective-permute-done | bytes 4128 | tf_op jit(solution)/shard_map/ppermute | solution.py:30
  86.6 7.2 %collective-permute-done.10 = f32[64,16]{0,1:T(8,128)S(1)} collective-permute-done((f32[64,16]{0,1:T(8,128)S(1)}, f32[64,16]{0,1:T(8,128)S(1)}, u32[]{:S(2)}, u32[]{:S(2)}) %collective-permute-start.10) | collective-permute-done | bytes 4128 | tf_op jit(solution)/shard_map/ppermute | solution.py:30
  93.9 7.2 %collective-permute-done.11 = f32[64,16]{0,1:T(8,128)S(1)} collective-permute-done((f32[64,16]{0,1:T(8,128)S(1)}, f32[64,16]{0,1:T(8,128)S(1)}, u32[]{:S(2)}, u32[]{:S(2)}) %collective-permute-start.11) | collective-permute-done | bytes 4128 | tf_op jit(solution)/shard_map/ppermute | solution.py:30
  101.1 7.2 %collective-permute-done.12 = f32[64,16]{0,1:T(8,128)S(1)} collective-permute-done((f32[64,16]{0,1:T(8,128)S(1)}, f32[64,16]{0,1:T(8,128)S(1)}, u32[]{:S(2)}, u32[]{:S(2)}) %collective-permute-start.12) | collective-permute-done | bytes 4128 | tf_op jit(solution)/shard_map/ppermute | solution.py:30
  108.4 7.2 %collective-permute-done.13 = f32[64,16]{0,1:T(8,128)S(1)} collective-permute-done((f32[64,16]{0,1:T(8,128)S(1)}, f32[64,16]{0,1:T(8,128)S(1)}, u32[]{:S(2)}, u32[]{:S(2)}) %collective-permute-start.13) | collective-permute-done | bytes 4128 | tf_op jit(solution)/shard_map/ppermute | solution.py:30
  115.6 7.2 %collective-permute-done.14 = f32[64,16]{0,1:T(8,128)S(1)} collective-permute-done((f32[64,16]{0,1:T(8,128)S(1)}, f32[64,16]{0,1:T(8,128)S(1)}, u32[]{:S(2)}, u32[]{:S(2)}) %collective-permute-start.14) | collective-permute-done | bytes 4128 | tf_op jit(solution)/shard_map/ppermute | solution.py:30
  123.1 6.5 %fusion.4 = f32[1024,512]{1,0:T(8,128)} fusion(bf16[1024,2048]{1,0:T(8,128)(2,1)} %all-gather.2.cloned.1.call-done, bf16[1,2048,512]{2,1,0:T(8,128)(2,1)} %param.11), kind=kOutput, calls=%fused_computation.3 | convolution fusion | flops 2147483648 | bytes 8388608 | tf_op jit(solution)/shard_map/dot_general | solution.py:36
  129.6 10.1 %multiply_convert_fusion = bf16[1024,2048]{1,0:T(8,128)(2,1)} fusion(f32[1024]{0:T(1024)S(1)} %bitcast.20, bf16[1,512,2048]{2,1,0:T(8,128)(2,1)S(1)} %copy-done, f32[1024,512]{1,0:T(8,128)} %fusion.4, bf16[1024,2048]{1,0:T(8,128)(2,1)} %all-gather.2.cloned.1.call-done, bf16[1,2048,512]{2,1,0:T(8,128)(2,1)} %param.10), kind=kOutput, calls=%fused_computation | convolution fusion | flops 4302307328 | bytes 14684160 | tf_op jit(solution)/shard_map/dot_general | solution.py:38
  139.8 7.8 %reduce-scatter.3.cloned.1.call-done = bf16[1024,1024]{1,0:T(8,128)(2,1)} async-done(((bf16[1024,2048]{1,0:T(8,128)(2,1)}), bf16[1024,1024]{1,0:T(8,128)(2,1)}) %reduce-scatter.3.cloned.1.call-update) | async-done | bytes 2097168 | tf_op jit(solution)/shard_map/reduce_scatter | solution.py:40
  147.6 85.1 %reduce-scatter.5.cloned.1.call-done = bf16[64,1024]{1,0:T(8,128)(2,1)} async-done(((bf16[1024,1024]{1,0:T(8,128)(2,1)}), bf16[64,1024]{1,0:T(8,128)(2,1)}) %reduce-scatter.5.cloned.1.call-update) | async-done | bytes 131088 | tf_op jit(solution)/shard_map/reduce_scatter | solution.py:41
  (28 shorter events, 1.8 us)
Async XLA Ops:
  6.5 123.1 %copy-start = (bf16[1,512,2048]{2,1,0:T(8,128)(2,1)S(1)}, bf16[1,512,2048]{2,1,0:T(8,128)(2,1)}, u32[]{:S(2)}) copy-start(bf16[1,512,2048]{2,1,0:T(8,128)(2,1)} %param.12) | copy-start | bytes 6291460
  6.5 116.5 %all-gather.2.cloned.1.call-start = ((), (), s32[]{:S(2)}) async-start(), calls=%async_computation.2 | async-start | bytes 4325376 | tf_op jit(solution)/shard_map/all_gather | solution.py:22
  9.4 138.2 %reduce-scatter.3.cloned.1.call-start = ((), (), s32[]{:S(2)}) async-start(), calls=%async_computation.3 | async-start | bytes 6291456 | tf_op jit(solution)/shard_map/reduce_scatter | solution.py:40
  12.3 8.6 %collective-permute-start = (f32[64,16]{0,1:T(8,128)S(1)}, f32[64,16]{0,1:T(8,128)S(1)}, u32[]{:S(2)}, u32[]{:S(2)}) collective-permute-start(f32[64,16]{0,1:T(8,128)S(1)} %bitcast_multiply_fusion), channel_id=1, source_target_pairs={{0,2},{2,4},{4,6},{6,8},{8,10},{10,12},{12,14},{14,16},{16,18},{18... | collective-permute-start | bytes 12296 | tf_op jit(solution)/shard_map/ppermute | solution.py:30
  20.9 7.3 %collective-permute-start.1 = (f32[64,16]{0,1:T(8,128)S(1)}, f32[64,16]{0,1:T(8,128)S(1)}, u32[]{:S(2)}, u32[]{:S(2)}) collective-permute-start(f32[64,16]{0,1:T(8,128)S(1)} %collective-permute-done), channel_id=1, source_target_pairs={{0,2},{2,4},{4,6},{6,8},{8,10},{10,12},{12,14},{14,16},{16,18},{18... | collective-permute-start | bytes 12296 | tf_op jit(solution)/shard_map/ppermute | solution.py:30
  28.1 7.3 %collective-permute-start.2 = (f32[64,16]{0,1:T(8,128)S(1)}, f32[64,16]{0,1:T(8,128)S(1)}, u32[]{:S(2)}, u32[]{:S(2)}) collective-permute-start(f32[64,16]{0,1:T(8,128)S(1)} %collective-permute-done.1), channel_id=1, source_target_pairs={{0,2},{2,4},{4,6},{6,8},{8,10},{10,12},{12,14},{14,16},{16,18},{18... | collective-permute-start | bytes 12296 | tf_op jit(solution)/shard_map/ppermute | solution.py:30
  35.4 7.4 %collective-permute-start.3 = (f32[64,16]{0,1:T(8,128)S(1)}, f32[64,16]{0,1:T(8,128)S(1)}, u32[]{:S(2)}, u32[]{:S(2)}) collective-permute-start(f32[64,16]{0,1:T(8,128)S(1)} %collective-permute-done.2), channel_id=1, source_target_pairs={{0,2},{2,4},{4,6},{6,8},{8,10},{10,12},{12,14},{14,16},{16,18},{18... | collective-permute-start | bytes 12296 | tf_op jit(solution)/shard_map/ppermute | solution.py:30
  42.8 7.3 %collective-permute-start.4 = (f32[64,16]{0,1:T(8,128)S(1)}, f32[64,16]{0,1:T(8,128)S(1)}, u32[]{:S(2)}, u32[]{:S(2)}) collective-permute-start(f32[64,16]{0,1:T(8,128)S(1)} %collective-permute-done.3), channel_id=1, source_target_pairs={{0,2},{2,4},{4,6},{6,8},{8,10},{10,12},{12,14},{14,16},{16,18},{18... | collective-permute-start | bytes 12296 | tf_op jit(solution)/shard_map/ppermute | solution.py:30
  50.1 7.2 %collective-permute-start.5 = (f32[64,16]{0,1:T(8,128)S(1)}, f32[64,16]{0,1:T(8,128)S(1)}, u32[]{:S(2)}, u32[]{:S(2)}) collective-permute-start(f32[64,16]{0,1:T(8,128)S(1)} %collective-permute-done.4), channel_id=1, source_target_pairs={{0,2},{2,4},{4,6},{6,8},{8,10},{10,12},{12,14},{14,16},{16,18},{18... | collective-permute-start | bytes 12296 | tf_op jit(solution)/shard_map/ppermute | solution.py:30
  57.3 7.5 %collective-permute-start.6 = (f32[64,16]{0,1:T(8,128)S(1)}, f32[64,16]{0,1:T(8,128)S(1)}, u32[]{:S(2)}, u32[]{:S(2)}) collective-permute-start(f32[64,16]{0,1:T(8,128)S(1)} %collective-permute-done.5), channel_id=1, source_target_pairs={{0,2},{2,4},{4,6},{6,8},{8,10},{10,12},{12,14},{14,16},{16,18},{18... | collective-permute-start | bytes 12296 | tf_op jit(solution)/shard_map/ppermute | solution.py:30
  64.9 7.3 %collective-permute-start.7 = (f32[64,16]{0,1:T(8,128)S(1)}, f32[64,16]{0,1:T(8,128)S(1)}, u32[]{:S(2)}, u32[]{:S(2)}) collective-permute-start(f32[64,16]{0,1:T(8,128)S(1)} %collective-permute-done.6), channel_id=1, source_target_pairs={{0,2},{2,4},{4,6},{6,8},{8,10},{10,12},{12,14},{14,16},{16,18},{18... | collective-permute-start | bytes 12296 | tf_op jit(solution)/shard_map/ppermute | solution.py:30
  72.1 7.2 %collective-permute-start.8 = (f32[64,16]{0,1:T(8,128)S(1)}, f32[64,16]{0,1:T(8,128)S(1)}, u32[]{:S(2)}, u32[]{:S(2)}) collective-permute-start(f32[64,16]{0,1:T(8,128)S(1)} %collective-permute-done.7), channel_id=1, source_target_pairs={{0,2},{2,4},{4,6},{6,8},{8,10},{10,12},{12,14},{14,16},{16,18},{18... | collective-permute-start | bytes 12296 | tf_op jit(solution)/shard_map/ppermute | solution.py:30
  79.4 7.2 %collective-permute-start.9 = (f32[64,16]{0,1:T(8,128)S(1)}, f32[64,16]{0,1:T(8,128)S(1)}, u32[]{:S(2)}, u32[]{:S(2)}) collective-permute-start(f32[64,16]{0,1:T(8,128)S(1)} %collective-permute-done.8), channel_id=1, source_target_pairs={{0,2},{2,4},{4,6},{6,8},{8,10},{10,12},{12,14},{14,16},{16,18},{18... | collective-permute-start | bytes 12296 | tf_op jit(solution)/shard_map/ppermute | solution.py:30
  86.6 7.2 %collective-permute-start.10 = (f32[64,16]{0,1:T(8,128)S(1)}, f32[64,16]{0,1:T(8,128)S(1)}, u32[]{:S(2)}, u32[]{:S(2)}) collective-permute-start(f32[64,16]{0,1:T(8,128)S(1)} %collective-permute-done.9), channel_id=1, source_target_pairs={{0,2},{2,4},{4,6},{6,8},{8,10},{10,12},{12,14},{14,16},{16,18},{18... | collective-permute-start | bytes 12296 | tf_op jit(solution)/shard_map/ppermute | solution.py:30
  93.9 7.2 %collective-permute-start.11 = (f32[64,16]{0,1:T(8,128)S(1)}, f32[64,16]{0,1:T(8,128)S(1)}, u32[]{:S(2)}, u32[]{:S(2)}) collective-permute-start(f32[64,16]{0,1:T(8,128)S(1)} %collective-permute-done.10), channel_id=1, source_target_pairs={{0,2},{2,4},{4,6},{6,8},{8,10},{10,12},{12,14},{14,16},{16,18},{18... | collective-permute-start | bytes 12296 | tf_op jit(solution)/shard_map/ppermute | solution.py:30
  101.1 7.2 %collective-permute-start.12 = (f32[64,16]{0,1:T(8,128)S(1)}, f32[64,16]{0,1:T(8,128)S(1)}, u32[]{:S(2)}, u32[]{:S(2)}) collective-permute-start(f32[64,16]{0,1:T(8,128)S(1)} %collective-permute-done.11), channel_id=1, source_target_pairs={{0,2},{2,4},{4,6},{6,8},{8,10},{10,12},{12,14},{14,16},{16,18},{18... | collective-permute-start | bytes 12296 | tf_op jit(solution)/shard_map/ppermute | solution.py:30
  108.4 7.2 %collective-permute-start.13 = (f32[64,16]{0,1:T(8,128)S(1)}, f32[64,16]{0,1:T(8,128)S(1)}, u32[]{:S(2)}, u32[]{:S(2)}) collective-permute-start(f32[64,16]{0,1:T(8,128)S(1)} %collective-permute-done.12), channel_id=1, source_target_pairs={{0,2},{2,4},{4,6},{6,8},{8,10},{10,12},{12,14},{14,16},{16,18},{18... | collective-permute-start | bytes 12296 | tf_op jit(solution)/shard_map/ppermute | solution.py:30
  115.6 7.2 %collective-permute-start.14 = (f32[64,16]{0,1:T(8,128)S(1)}, f32[64,16]{0,1:T(8,128)S(1)}, u32[]{:S(2)}, u32[]{:S(2)}) collective-permute-start(f32[64,16]{0,1:T(8,128)S(1)} %collective-permute-done.13), channel_id=1, source_target_pairs={{0,2},{2,4},{4,6},{6,8},{8,10},{10,12},{12,14},{14,16},{16,18},{18... | collective-permute-start | bytes 12296 | tf_op jit(solution)/shard_map/ppermute | solution.py:30
  139.7 93.0 %reduce-scatter.5.cloned.1.call-start = ((), (), s32[]{:S(2)}) async-start(), calls=%async_computation.4 | async-start | bytes 2228224 | tf_op jit(solution)/shard_map/reduce_scatter | solution.py:41
Sparse Core Ops, SparseCore 0:
  10.2 64.7 all-gather.1
  139.9 7.7 reduce-scatter.2
  149.9 82.8 reduce-scatter.4
